TPU v7x, 512 devices: a whole 4x8x8 slice. The times are simulated.
512 devices in a mesh: fs: 64 (over z, y), tp: 8 (over x, core).
Axes of the slice: x: 4, y: 8, z: 8, core: 2. Of those that a mesh axis runs over, the one named last changes fastest.
Arguments:
- prompt: bfloat16 [20480, 2048], P('fs', 'tp'), may hold values from -6 to 6
- norm_gain: float32 [2048], P('fs'), may hold values from 0.1 to 1.9
- gate_master: float32 [2048, 3072], P('fs', 'tp'), may hold values from -0.125 to 0.125
- up_master: float32 [2048, 3072], P('fs', 'tp'), may hold values from -0.125 to 0.125
- down_master: float32 [2048, 3072], P('fs', 'tp'), may hold values from -0.109375 to 0.109375
Outputs:
- gate_new: bfloat16 [3072, 2048], P('tp')
- up_new: bfloat16 [3072, 2048], P('tp')
- down_new: bfloat16 [3072, 2048], P('tp')
- mixed: bfloat16 [2048, 20480], P('tp', 'fs')
All inputs are finite; a program needn't handle non-finite values.
Results may differ from a plain program's by a relative error of at most 0.0082.
Values may be sent and summed in bfloat16 or wider, within the bound.
No kernel may reach another device: no remote copies, remote signals or barrier semaphores. Data moves between devices by JAX's collectives and lax.ppermute only.
A program may use at most 64 MiB of HBM per device.

v0:
```python
import jax
import jax.numpy as jnp
from jax import lax
from jax.sharding import PartitionSpec as P


def laid_out(parts, dim):
    parts = jnp.moveaxis(parts, 0, dim)
    shape = parts.shape
    return parts.reshape(*shape[:dim], shape[dim] * shape[dim + 1], *shape[dim + 2 :])


def sent_to_all(array, axis):
    copies = jnp.broadcast_to(array, (lax.axis_size(axis), *array.shape))
    return lax.all_to_all(copies, axis, split_axis=0, concat_axis=0, tiled=True)


def gathered_copies(array, axis, dim):
    return laid_out(sent_to_all(array, axis), dim)


def gather_turned(arrays, axis, dims):
    turned = [jnp.moveaxis(a, dim, 0) for a, dim in zip(arrays, dims)]
    widths = [t[0].size for t in turned]
    both = jnp.concatenate([t.reshape(-1, w) for t, w in zip(turned, widths)], axis=1)
    filled = lax.all_gather(both, axis, axis=0, tiled=True)
    parts = jnp.split(filled, [sum(widths[:k]) for k in range(1, len(widths))], axis=1)
    return tuple(
        (
            jnp.moveaxis(b.reshape(-1, *t.shape[1:]), 0, dim)
            for b, t, dim in zip(parts, turned, dims)
        )
    )


def cut_along(array, dim, size):
    before, after = (array.shape[:dim], array.shape[dim + 1 :])
    return jnp.moveaxis(array.reshape(*before, size, -1, *after), dim, 0)


def sent_and_summed(array, axis, dim):
    parts = cut_along(array, dim, lax.axis_size(axis))
    arrived = lax.all_to_all(parts, axis, split_axis=0, concat_axis=0, tiled=True)
    return arrived.astype(jnp.float32).sum(axis=0)


def on_device(prompt, norm_gain, gate_master, up_master, down_master):
    gain_col = norm_gain[:, None]
    gate_low = (gate_master * gain_col).astype(jnp.bfloat16).T
    up_low = (up_master * gain_col).astype(jnp.bfloat16).T
    down_low = down_master.astype(jnp.bfloat16).T
    whole = gathered_copies(prompt, "tp", 1)
    values = whole.astype(jnp.float32)
    normed = (values * lax.rsqrt(jnp.mean(values * values, axis=1, keepdims=True) + 1e-06)).astype(
        jnp.bfloat16
    )
    contract = (((1,), (1,)), ((), ()))
    gate_new, up_new, down_new = gather_turned((gate_low, up_low, down_low), "fs", (1, 1, 1))
    gate = lax.dot_general(normed, gate_new, contract, preferred_element_type=jnp.float32)
    up = lax.dot_general(normed, up_new, contract, preferred_element_type=jnp.float32)
    hidden = (jax.nn.silu(gate) * up).astype(jnp.bfloat16)
    mixed = sent_and_summed(
        lax.dot_general(
            down_new, hidden, (((0,), (1,)), ((), ())), preferred_element_type=jnp.float32
        ).astype(jnp.bfloat16),
        "tp",
        0,
    )
    return (gate_new, up_new, down_new, mixed.astype(jnp.bfloat16))


def solution(mesh):
    placed = (P("fs", "tp"), P("fs"), P("fs", "tp"), P("fs", "tp"), P("fs", "tp"))
    return jax.shard_map(
        on_device,
        mesh=mesh,
        in_specs=placed,
        out_specs=(P("tp", None), P("tp", None), P("tp", None), P("tp", "fs")),
        check_vma=False,
    )
```

profile of v0, /device:TPU:1, one launch (start us, length us, event | category | flops | bytes accessed | tf_op | source)
XLA Modules:
  0.0 145.5 jit_solution(8326352939495786494)
XLA Ops:
  7.2 0.0 all-gather.2.cloned.1.call-start
  7.2 0.8 convert_element_type.35
  8.0 0.9 multiply_convert_fusion.2
  8.9 0.6 pad_maximum_fusion
  9.6 0.0 all-gather.2.cloned.1.call-update
  9.6 1.0 broadcast_in_dim.2
  10.6 27.0 %all_to_all.10 = bf16[8,320,256]{2,1,0:T(8,128)(2,1)S(1)} all-to-all(bf16[8,320,256]{2,1,0:T(8,128)(2,1)S(1)} %broadcast_in_dim.2), channel_id=1, replica_groups=mesh['fs'=64,'tp'=8] {'tp'}, dimensions={0} | all-to-all | bytes 2621440 | tf_op jit(solution)/shard_map/all_to_all | solution.py:15
  37.6 0.2 convert_bitcast_fusion
  37.8 0.3 copy.21
  38.2 0.4 fusion
  38.6 61.7 %all-gather.2.cloned.1.call-done = bf16[2048,1152]{1,0:T(8,128)(2,1)} async-done(((bf16[32,1152]{1,0:T(8,128)(2,1)}), bf16[2048,1152]{1,0:T(8,128)(2,1)}) %all-gather.2.cloned.1.call-update) | async-done | bytes 4718608 | tf_op jit(solution)/shard_map/all_gather | solution.py:26
  100.3 2.3 %fusion.4 = f32[320,384]{1,0:T(8,128)S(1)} fusion(bf16[2048,1152]{1,0:T(8,128)(2,1)} %all-gather.2.cloned.1.call-done, f32[320,2048]{1,0:T(8,128)S(1)} %bitcast.14, f32[320]{0:T(512)S(1)} %add_rsqrt_fusion), kind=kOutput, calls=%fused_computation.10 | convolution fusion | flops 504627200 | bytes 4687104 | tf_op jit(solution)/shard_map/dot_general | solution.py:59
  102.6 4.6 %convolution_convert_fusion = bf16[2048,320]{0,1:T(8,128)(2,1)} fusion(bf16[2048,1152]{1,0:T(8,128)(2,1)} %all-gather.2.cloned.1.call-done, f32[320,384]{1,0:T(8,128)S(1)} %fusion.4, f32[320,2048]{1,0:T(8,128)S(1)} %bitcast.15, f32[320]{0:T(512)S(1)} %add_rsqrt_fusion), kind=kOutput, calls=%fused_computation.2 | convolution fusion | flops 1009336320 | bytes 7570688 | tf_op jit(solution)/shard_map/dot_general | solution.py:63
  107.2 2.5 %copy.23 = bf16[40,8,8,256]{3,2,0,1:T(8,128)(2,1)} copy(bf16[40,8,8,256]{3,2,1,0:T(8,128)(2,1)} %bitcast.16) | data formatting | bytes 2621440 | tf_op jit(solution)/shard_map/reshape | solution.py:38
  109.7 8.9 %all-to-all-start.1 = ((bf16[8,256,320]{1,2,0:T(8,128)(2,1)}), bf16[8,256,320]{1,2,0:T(8,128)(2,1)}, u32[]{:S(2)}, u32[]{:S(2)}) async-start(bf16[8,256,320]{1,2,0:T(8,128)(2,1)} %bitcast.13), calls=%async_computation.1 | async-start | bytes 2621440 | tf_op jit(solution)/shard_map/all_to_all | solution.py:43
  118.6 4.0 %slice_bitcast_fusion = (bf16[384,2048]{0,1:T(8,128)(2,1)}, bf16[384,2048]{0,1:T(8,128)(2,1)S(1)}, bf16[384,2048]{0,1:T(8,128)(2,1)S(1)}) fusion(bf16[2048,1152]{1,0:T(8,128)(2,1)} %all-gather.2.cloned.1.call-done), kind=kLoop, calls=%fused_computation.6 | loop fusion | bytes 9437184 | tf_op jit(solution)/shard_map/transpose | solution.py:30
  122.6 2.6 %copy.19 = bf16[384,2048]{1,0:T(8,128)(2,1)} copy(bf16[384,2048]{0,1:T(8,128)(2,1)} %get-tuple-element.8) | data formatting | bytes 3145728
  125.2 1.6 %copy.18 = bf16[384,2048]{1,0:T(8,128)(2,1)} copy(bf16[384,2048]{0,1:T(8,128)(2,1)S(1)} %get-tuple-element.9) | data formatting | bytes 3145728
  126.8 1.6 %copy.17 = bf16[384,2048]{1,0:T(8,128)(2,1)} copy(bf16[384,2048]{0,1:T(8,128)(2,1)S(1)} %get-tuple-element.10) | data formatting | bytes 3145728
  128.4 8.1 %all-to-all-done.1 = bf16[8,256,320]{1,2,0:T(8,128)(2,1)} async-done(((bf16[8,256,320]{1,2,0:T(8,128)(2,1)}), bf16[8,256,320]{1,2,0:T(8,128)(2,1)}, u32[]{:S(2)}, u32[]{:S(2)}) %all-to-all-start.1) | async-done | bytes 1310752 | tf_op jit(solution)/shard_map/all_to_all | solution.py:43
  136.5 2.2 %reduce_sum.22 = bf16[256,320]{0,1:T(8,128)(2,1)} reduce(bf16[8,256,320]{1,2,0:T(8,128)(2,1)} %all-to-all-done.1, bf16[]{:T(256)} %constant.11.clone.1), dimensions={0}, to_apply=%region_1.2 | reduce | flops 573440 | bytes 1474562 | tf_op jit(solution)/shard_map/reduce_sum | solution.py:44
  (1 shorter events, 0.0 us)
Async XLA Ops:
  7.2 93.1 %all-gather.2.cloned.1.call-start = ((), (), s32[]{:S(2)}) async-start(), calls=%async_computation.2 | async-start | bytes 4792320 | tf_op jit(solution)/shard_map/all_gather | solution.py:26
  109.7 26.8 %all-to-all-start.1 = ((bf16[8,256,320]{1,2,0:T(8,128)(2,1)}), bf16[8,256,320]{1,2,0:T(8,128)(2,1)}, u32[]{:S(2)}, u32[]{:S(2)}) async-start(bf16[8,256,320]{1,2,0:T(8,128)(2,1)} %bitcast.13), calls=%async_computation.1 | async-start | bytes 2621440 | tf_op jit(solution)/shard_map/all_to_all | solution.py:43
Sparse Core Ops, SparseCore 0:
  11.6 88.6 all-gather.1
where the time goes:
time: 146 us
  waiting for transfers between devices  69.8 us (48%)
  blocking collectives  27 us (18%)
  between operations  14.1 us (10%)
  local copies, waits for them, and re-layouts  13.7 us (9%)
  starting transfers between devices  8.97 us (6%)
  matrix products  6.86 us (5%)
  other arithmetic  5.16 us (4%)
    all_gather x1, waiting for transfers between devices, gather_turned(): filled = lax.all_gather(both, axis, axis=0, tiled=True)  61.7 us
    all_to_all x1, blocking collectives, sent_to_all(): return lax.all_to_all(copies, axis, split_axis=0, concat_axis=0, tiled=True)  27 us
    all_to_all x1, starting transfers between devices, sent_and_summed(): lax.all_to_all(parts, axis, split_axis=0, concat_axis=0, tiled=True)  8.93 us
    all_to_all x1, waiting for transfers between devices, sent_and_summed(): lax.all_to_all(parts, axis, split_axis=0, concat_axis=0, tiled=True)  8.07 us
    unnamed x3, local copies, waits for them, and re-layouts  5.81 us
    dot_general x1, matrix products, on_device(): lax.dot_general(down_new, hidden, (((0,), (1,)), ((), ())), preferred_ele...  4.58 us
    transpose x1, local copies, waits for them, and re-layouts, gather_turned(): jnp.moveaxis(b.reshape(-1, *t.shape[1:]), 0, dim)  4 us
  transfers between devices with their start and end apart: 2, of which 2 were waited for; matrix products, arithmetic and copies ran while one was open for 8% of the time, Pallas kernels for 0%

commit v1 on v0

--- a/solution.py
+++ b/solution.py
@@ -23,7 +23,14 @@
     turned = [jnp.moveaxis(a, dim, 0) for a, dim in zip(arrays, dims)]
     widths = [t[0].size for t in turned]
     both = jnp.concatenate([t.reshape(-1, w) for t, w in zip(turned, widths)], axis=1)
-    filled = lax.all_gather(both, axis, axis=0, tiled=True)
+
+    def set_thing_now(row_data, named_axis):
+        return jnp.concatenate(
+            lax.all_to_all(jnp.stack([row_data] * lax.axis_size(named_axis), 0), named_axis, 0, 0),
+            0,
+        )
+
+    filled = set_thing_now(both, axis)
     parts = jnp.split(filled, [sum(widths[:k]) for k in range(1, len(widths))], axis=1)
     return tuple(
         (

time: 146 us -> 228 us (1.56)
  the two profiles are of different devices: /device:TPU:1 before, /device:TPU:40 now
where the time goes in v1:
time: 228 us; the launch traced here: 227 us
  waiting for transfers between devices  170 us (75%)
  starting transfers between devices  28.1 us (12%)
  local copies, waits for them, and re-layouts  18.3 us (8%)
  matrix products  6.86 us (3%)
  other arithmetic  2.89 us (1%)
    all_to_all x1, waiting for transfers between devices, set_thing_now(): lax.all_to_all(jnp.stack([row_data] * lax.axis_size(named_axis), 0), name...  143 us
    all_to_all x1, waiting for transfers between devices, sent_to_all(): return lax.all_to_all(copies, axis, split_axis=0, concat_axis=0, tiled=True)  18.6 us
    all_to_all x1, starting transfers between devices, set_thing_now(): lax.all_to_all(jnp.stack([row_data] * lax.axis_size(named_axis), 0), name...  16.3 us
    all_to_all x1, waiting for transfers between devices, sent_and_summed(): lax.all_to_all(parts, axis, split_axis=0, concat_axis=0, tiled=True)  9.04 us
    all_to_all x1, starting transfers between devices, sent_and_summed(): lax.all_to_all(parts, axis, split_axis=0, concat_axis=0, tiled=True)  7.34 us
    unnamed x15, local copies, waits for them, and re-layouts  6.78 us
    dot_general x1, matrix products, on_device(): lax.dot_general(down_new, hidden, (((0,), (1,)), ((), ())), preferred_ele...  4.58 us
  transfers between devices with their start and end apart: 3, of which 3 were waited for; matrix products, arithmetic and copies ran while one was open for 5% of the time, Pallas kernels for 0%

profile of v1, /device:TPU:40, one launch (start us, length us, event | category | flops | bytes accessed | tf_op | source)
XLA Modules:
  0.0 227.1 jit_solution(6413101152671446926)
XLA Ops:
  0.6 2.1 broadcast_in_dim.2
  2.7 4.4 %all-to-all-start.1 = ((bf16[8,320,256]{2,1,0:T(8,128)(2,1)}), bf16[8,320,256]{2,1,0:T(8,128)(2,1)S(1)}, u32[]{:S(2)}, u32[]{:S(2)}) async-start(bf16[8,320,256]{2,1,0:T(8,128)(2,1)} %broadcast_in_dim.2), calls=%async_computation.1 | async-start | bytes 2621440 | tf_op jit(solution)/shard_map/all_to_all | solution.py:15
  7.1 0.0 copy-done.2
  7.2 0.0 copy-done.3
  7.2 0.1 multiply_convert_fusion.2
  7.3 18.6 %all-to-all-done.1 = bf16[8,320,256]{2,1,0:T(8,128)(2,1)S(1)} async-done(((bf16[8,320,256]{2,1,0:T(8,128)(2,1)}), bf16[8,320,256]{2,1,0:T(8,128)(2,1)S(1)}, u32[]{:S(2)}, u32[]{:S(2)}) %all-to-all-start.1) | async-done | bytes 1310752 | tf_op jit(solution)/shard_map/all_to_all | solution.py:15
  25.9 2.6 %stack.2 = bf16[64,32,1152]{2,1,0:T(8,128)(2,1)} broadcast(bf16[32,1152]{1,0:T(8,128)(2,1)S(1)} %pad_maximum_fusion), dimensions={1,2} | broadcast | bytes 4792320 | tf_op jit(solution)/shard_map/stack | solution.py:29
  28.5 16.3 %all-to-all-start = ((bf16[64,32,1152]{2,1,0:T(8,128)(2,1)}), bf16[64,32,1152]{2,1,0:T(8,128)(2,1)}, u32[]{:S(2)}, u32[]{:S(2)}) async-start(bf16[64,32,1152]{2,1,0:T(8,128)(2,1)} %stack.2), calls=%async_computation | async-start | bytes 9437184 | tf_op jit(solution)/shard_map/all_to_all | solution.py:29
  44.8 0.2 convert_bitcast_fusion
  45.0 0.0 copy-start.1
  45.1 0.3 copy.19
  45.4 0.9 copy-done.1
  46.4 0.4 fusion
  46.7 142.7 %all-to-all-done = bf16[64,32,1152]{2,1,0:T(8,128)(2,1)} async-done(((bf16[64,32,1152]{2,1,0:T(8,128)(2,1)}), bf16[64,32,1152]{2,1,0:T(8,128)(2,1)}, u32[]{:S(2)}, u32[]{:S(2)}) %all-to-all-start) | async-done | bytes 4718624 | tf_op jit(solution)/shard_map/all_to_all | solution.py:29
  189.4 2.3 %fusion.4 = f32[320,384]{1,0:T(8,128)S(1)} fusion(bf16[2048,1152]{1,0:T(8,128)(2,1)} %bitcast, f32[320,2048]{1,0:T(8,128)S(1)} %bitcast.15, f32[320]{0:T(512)S(1)} %add_rsqrt_fusion), kind=kOutput, calls=%fused_computation.10 | convolution fusion | flops 504627200 | bytes 4687104 | tf_op jit(solution)/shard_map/dot_general | solution.py:66
  191.7 4.6 %convolution_convert_fusion = bf16[2048,320]{0,1:T(8,128)(2,1)} fusion(bf16[2048,1152]{1,0:T(8,128)(2,1)} %bitcast, f32[320,384]{1,0:T(8,128)S(1)} %fusion.4, f32[320,2048]{1,0:T(8,128)S(1)} %bitcast.16, f32[320]{0:T(512)S(1)} %add_rsqrt_fusion), kind=kOutput, calls=%fused_computation.2 | convolution fusion | flops 1009336320 | bytes 7570688 | tf_op jit(solution)/shard_map/dot_general | solution.py:70
  196.3 2.5 %copy.21 = bf16[40,8,8,256]{3,2,0,1:T(8,128)(2,1)} copy(bf16[40,8,8,256]{3,2,1,0:T(8,128)(2,1)} %bitcast.17) | data formatting | bytes 2621440 | tf_op jit(solution)/shard_map/reshape | solution.py:45
  198.8 7.3 %all-to-all-start.2 = ((bf16[8,256,320]{1,2,0:T(8,128)(2,1)}), bf16[8,256,320]{1,2,0:T(8,128)(2,1)}, u32[]{:S(2)}, u32[]{:S(2)}) async-start(bf16[8,256,320]{1,2,0:T(8,128)(2,1)} %bitcast.14), calls=%async_computation.2 | async-start | bytes 2621440 | tf_op jit(solution)/shard_map/all_to_all | solution.py:50
  206.1 4.0 %slice_bitcast_fusion = (bf16[384,2048]{0,1:T(8,128)(2,1)S(1)}, bf16[384,2048]{0,1:T(8,128)(2,1)S(1)}, bf16[384,2048]{0,1:T(8,128)(2,1)}) fusion(bf16[2048,1152]{1,0:T(8,128)(2,1)} %bitcast), kind=kLoop, calls=%fused_computation.6 | loop fusion | bytes 9437184 | tf_op jit(solution)/shard_map/transpose | solution.py:37
  210.1 2.6 %copy.15 = bf16[384,2048]{1,0:T(8,128)(2,1)} copy(bf16[384,2048]{0,1:T(8,128)(2,1)} %get-tuple-element.14) | data formatting | bytes 3145728
  212.7 1.6 copy.16
  214.3 1.6 copy.17
  215.9 9.0 %all-to-all-done.2 = bf16[8,256,320]{1,2,0:T(8,128)(2,1)} async-done(((bf16[8,256,320]{1,2,0:T(8,128)(2,1)}), bf16[8,256,320]{1,2,0:T(8,128)(2,1)}, u32[]{:S(2)}, u32[]{:S(2)}) %all-to-all-start.2) | async-done | bytes 1310752 | tf_op jit(solution)/shard_map/all_to_all | solution.py:50
  224.9 2.2 reduce_sum.22
  (11 shorter events, 0.0 us)
Async XLA Ops:
  2.7 4.5 %copy-start.2 = (f32[32,384]{1,0:T(8,128)S(1)}, f32[32,384]{1,0:T(8,128)}, u32[]{:S(2)}) copy-start(f32[32,384]{1,0:T(8,128)} %param.9) | copy-start | bytes 147460
  2.7 4.5 %copy-start.3 = (f32[32,384]{1,0:T(8,128)S(1)}, f32[32,384]{1,0:T(8,128)}, u32[]{:S(2)}) copy-start(f32[32,384]{1,0:T(8,128)} %param.7) | copy-start | bytes 147460
  2.7 4.5 %copy-start.4 = (f32[32,384]{1,0:T(8,128)S(1)}, f32[32,384]{1,0:T(8,128)}, u32[]{:S(2)}) copy-start(f32[32,384]{1,0:T(8,128)} %param.8) | copy-start | bytes 147460
  2.7 4.5 %copy-start.5 = (f32[32]{0:T(128)S(1)}, f32[32]{0:T(128)}, u32[]{:S(2)}) copy-start(f32[32]{0:T(128)} %param.6) | copy-start | bytes 388
  2.7 23.2 %all-to-all-start.1 = ((bf16[8,320,256]{2,1,0:T(8,128)(2,1)}), bf16[8,320,256]{2,1,0:T(8,128)(2,1)S(1)}, u32[]{:S(2)}, u32[]{:S(2)}) async-start(bf16[8,320,256]{2,1,0:T(8,128)(2,1)} %broadcast_in_dim.2), calls=%async_computation.1 | async-start | bytes 2621440 | tf_op jit(solution)/shard_map/all_to_all | solution.py:15
  25.9 18.9 %copy-start = (bf16[8,320,256]{2,1,0:T(8,128)(2,1)}, bf16[8,320,256]{2,1,0:T(8,128)(2,1)S(1)}, u32[]{:S(2)}) copy-start(bf16[8,320,256]{2,1,0:T(8,128)(2,1)S(1)} %all-to-all-done.1) | copy-start | bytes 3932164
  28.5 160.9 %all-to-all-start = ((bf16[64,32,1152]{2,1,0:T(8,128)(2,1)}), bf16[64,32,1152]{2,1,0:T(8,128)(2,1)}, u32[]{:S(2)}, u32[]{:S(2)}) async-start(bf16[64,32,1152]{2,1,0:T(8,128)(2,1)} %stack.2), calls=%async_computation | async-start | bytes 9437184 | tf_op jit(solution)/shard_map/all_to_all | solution.py:29
  45.0 1.3 copy-start.1
  198.8 26.2 %all-to-all-start.2 = ((bf16[8,256,320]{1,2,0:T(8,128)(2,1)}), bf16[8,256,320]{1,2,0:T(8,128)(2,1)}, u32[]{:S(2)}, u32[]{:S(2)}) async-start(bf16[8,256,320]{1,2,0:T(8,128)(2,1)} %bitcast.14), calls=%async_computation.2 | async-start | bytes 2621440 | tf_op jit(solution)/shard_map/all_to_all | solution.py:50
